TPU v7x, 32 devices: a whole 2x2x4 slice. The times are simulated.
32 devices in a mesh: rep: 2 (over x), fs: 8 (over z, y), tp: 2 (over core).
Axes of the slice: x: 2, y: 2, z: 4, core: 2. Of those that a mesh axis runs over, the one named last changes fastest.
Arguments:
- tokens: bfloat16 [10240, 2048], P(('rep', 'fs', 'tp')), may hold values from -6 to 6
- mix_gain: float32 [2048], replicated, may hold values from 0.1 to 1.9
- w_bgate: bfloat16 [2048, 2048], P('fs', 'tp'), may hold values from -0.125 to 0.125
- w_cgate: bfloat16 [2048, 2048], P('fs', 'tp'), may hold values from -0.125 to 0.125
- w_value: bfloat16 [2048, 2048], P('fs', 'tp'), may hold values from -0.125 to 0.125
- conv_taps: float32 [3, 2048], replicated, may hold values from -3 to 3
- w_mixout: bfloat16 [2048, 2048], P('tp', 'fs'), may hold values from -0.125 to 0.125
- mlp_gain: float32 [2048], replicated, may hold values from 0.1 to 1.9
- w_gate: bfloat16 [2048, 2816], P('fs', 'tp'), may hold values from -0.125 to 0.125
- w_up: bfloat16 [2048, 2816], P('fs', 'tp'), may hold values from -0.125 to 0.125
- w_down: bfloat16 [2816, 2048], P('tp', 'fs'), may hold values from -0.109375 to 0.109375
Outputs:
- block_out: bfloat16 [10240, 2048], P(('rep', 'fs', 'tp'))
All inputs are finite; a program needn't handle non-finite values.
Results may differ from a plain program's by a relative error of at most 0.0085.
Values may be sent and summed in bfloat16 or wider, within the bound.
A program may use at most 128 MiB of HBM per device.

v0:
```python
import functools

import jax
import jax.numpy as jnp
from jax import lax
from jax.experimental import pallas as pl
from jax.experimental.pallas import tpu as pltpu
from jax.sharding import PartitionSpec as P


def rms_scale(matrix, gain):
    values = matrix.astype(jnp.float32)
    factor = lax.rsqrt(jnp.mean(values * values, axis=-1, keepdims=True) + 1e-06)
    return values * factor * gain


def causal_taps(mixed, filters):
    length = mixed.shape[-2]
    padded = jnp.pad(mixed, [(2, 0), (0, 0)])
    return (
        filters[0] * padded[0:length]
        + filters[1] * padded[1 : length + 1]
        + filters[2] * padded[2 : length + 2]
    )


def swap(array, axis):
    return lax.ppermute(array, axis, [(0, 1), (1, 0)])


def half(array, axis, part):
    size = array.shape[axis] // 2
    return lax.dynamic_slice_in_dim(array, part * size, size, axis)


def build(n_fs):
    ring = [(i, (i + 2) % n_fs) for i in range(n_fs)]
    pair = [(i, i ^ 1) for i in range(n_fs)]
    steps = n_fs // 2

    def ring_first(block):
        blocks = []
        for step in range(steps):
            blocks += [block, lax.ppermute(block, "fs", pair)]
            if step < steps - 1:
                block = lax.ppermute(block, "fs", ring)
        return blocks

    def pair_first(block):
        mate = lax.ppermute(block, "fs", pair)
        blocks = []
        for step in range(steps):
            blocks += [block, mate]
            if step < steps - 1:
                block = lax.ppermute(block, "fs", ring)
                mate = lax.ppermute(mate, "fs", ring)
        return blocks

    def on_device(
        tokens, mix_gain, w_bgate, w_cgate, w_value, conv_taps, w_mixout, mlp_gain, w_gate, w_up, w_down
    ):
        rep, fs, tp = (lax.axis_index(name) for name in ("rep", "fs", "tp"))
        width = tokens.shape[1] // n_fs

        def arrival_order(array):
            order = [((fs ^ j) - 2 * s + n_fs) % n_fs for s in range(steps) for j in range(2)]
            return jnp.concatenate(
                [lax.dynamic_slice_in_dim(array, k * width, width, array.ndim - 1) for k in order],
                axis=-1,
            )

        def global_order(array):
            places = []
            for k in range(n_fs):
                j = (fs ^ k) & 1
                places.append((((fs ^ j) - k + n_fs) % n_fs) + j)
            return jnp.concatenate(
                [lax.dynamic_slice_in_dim(array, k * width, width, array.ndim - 1) for k in places],
                axis=-1,
            )

        def sequence(rows):
            other = swap(rows, "tp")
            return jnp.concatenate(
                [jnp.where(tp == 0, rows, other), jnp.where(tp == 0, other, rows)], axis=0
            )

        def both_sequences(rows):
            away = swap(rows, "rep")
            return sequence(rows), sequence(away)

        def chip_sum(partial):
            other = swap(half(partial, 0, 1 - tp), "tp")
            return half(partial, 0, tp).astype(jnp.float32) + other.astype(jnp.float32)

        def project_out(mine, theirs, blocks, group):
            sums = []
            for start in range(0, len(blocks), group):
                weight = jnp.concatenate(blocks[start : start + group], axis=1)
                outs = []
                for rows in (theirs, mine):
                    outs.append(
                        jnp.dot(rows, weight, preferred_element_type=jnp.float32).astype(
                            jnp.bfloat16
                        )
                    )
                away = swap(chip_sum(outs[0]).astype(jnp.bfloat16), "rep")
                sums.append(chip_sum(outs[1]) + away.astype(jnp.float32))
            return jnp.concatenate(sums, axis=1)

        w_in = jnp.concatenate([half(w, 1, rep) for w in (w_bgate, w_cgate, w_value)], axis=1)
        w_gu = jnp.concatenate([half(w, 1, rep) for w in (w_gate, w_up)], axis=1)
        in_blocks = ring_first(w_in)
        out_blocks = ring_first(half(w_mixout, 0, rep))
        upper, lower = jnp.split(w_gu, 2, axis=0)
        gu_blocks = [part for both in zip(pair_first(upper), ring_first(lower)) for part in both]
        down_blocks = ring_first(half(w_down, 0, rep))

        channels = w_in.shape[1] // 3
        taps = lax.dynamic_slice_in_dim(conv_taps, (tp * 2 + rep) * channels, channels, 1)
        local = arrival_order(tokens)

        def mix(normed, weight):
            projected = jnp.dot(normed, weight, preferred_element_type=jnp.float32).astype(
                jnp.bfloat16
            )
            b_proj, c_proj, u_proj = (
                projected[:, k * channels : (k + 1) * channels].astype(jnp.float32)
                for k in range(3)
            )
            return (b_proj * causal_taps(c_proj * u_proj, taps)).astype(jnp.bfloat16)

        mine, theirs = both_sequences(rms_scale(local, arrival_order(mix_gain)).astype(jnp.bfloat16))
        weight = jnp.concatenate(in_blocks, axis=0)
        theirs, mine = mix(theirs, weight), mix(mine, weight)
        mixed = project_out(mine, theirs, out_blocks, 2)
        residual = local.astype(jnp.float32) + mixed

        units = w_gu.shape[1] // 2

        def feed(normed, weight):
            both = jnp.dot(normed, weight, preferred_element_type=jnp.float32)
            return (jax.nn.silu(both[:, :units]) * both[:, units:]).astype(jnp.bfloat16)

        mine, theirs = both_sequences(rms_scale(residual, arrival_order(mlp_gain)).astype(jnp.bfloat16))
        weight = jnp.concatenate(gu_blocks, axis=0)
        theirs, mine = feed(theirs, weight), feed(mine, weight)
        down = project_out(mine, theirs, down_blocks, 2)
        return global_order((residual + 0.5 * down).astype(jnp.bfloat16))

    return on_device


MESH = pl.DeviceIdType.MESH
STRIP = 16
LANES = 128
INPUT, OUT, GU, DN = (0, 1, 2), (3,), (4,), (5,)


def f32(value):
    return value.astype(jnp.float32)


def mxu(left, right):
    return jnp.dot(left, right, preferred_element_type=jnp.float32)


def kernel(
    n_z,
    tok_hbm, gain_one, wb_hbm, wc_hbm, wu_hbm, taps, wo_hbm, gain_two, wgu_hbm, wd_hbm,
    out_hbm,
    wb, wc, wu, wo, wgu, wd,
    tok, normed, gated, part, theirs, outgo, income, res, normed_two, hidden,
    part_two, theirs_two, outgo_two, income_two, final,
    tail,
    load_sem, y_send, y_recv, zown_send, zfwd_send, z_recv, x_send, x_recv,
    one_send, one_recv, mix_send, mix_recv, mid_send, mid_recv, two_send, two_recv, store_sem,
):
    rep, fs, tp = (lax.axis_index(name) for name in ("rep", "fs", "tp"))
    z, y = lax.div(fs, 2), lax.rem(fs, 2)
    rows, _ = tok.shape
    sub = rows // 2
    depth = wb_hbm.shape[0]
    channels = wb.shape[1]
    pair_units = wgu.shape[1]
    units = pair_units // 2
    width = wo.shape[2]
    n_fs = 2 * n_z
    core = (rep, fs, 1 - tp)
    mate = (rep, z * 2 + 1 - y, tp)
    twin = (1 - rep, fs, tp)

    def along(position):
        return (rep, position * 2 + y, tp)

    def kth(k):
        near = jnp.minimum(z, n_z - 1 - z)
        both = z + ((k + 1) // 2) * (1 if k % 2 == 0 else -1)
        far = jnp.where(z < n_z - 1 - z, z + (k - near), z - (k - near))
        return jnp.where(k <= 2 * near, both, far)

    def line(rr, position):
        return position * 2 + (y if rr == 0 else 1 - y)

    def source(t, half, piece=None):
        parts = 2 if piece is None else 1
        first = 0 if piece is None else piece
        if t in OUT + DN:
            ref = (wo_hbm, wd_hbm)[t == 5]
            size = ref.shape[0] // 4
            return ref.at[pl.ds(pl.multiple_of((half * 2 + first) * size, 16), parts * size), :]
        ref = (wb_hbm, wc_hbm, wu_hbm, None, wgu_hbm)[t]
        cols = pair_units if t == 4 else channels
        size = depth // 2
        return ref.at[
            pl.ds(pl.multiple_of(first * size, 16), parts * size),
            pl.ds(pl.multiple_of(half * cols, 128), cols),
        ]

    def slot(t, index, piece=None):
        parts = 2 if piece is None else 1
        first = 0 if piece is None else piece
        if t in OUT + DN:
            ref = (wo, wd)[t == 5]
            size = ref.shape[1] // 2
            return ref.at[index, pl.ds(pl.multiple_of(first * size, 16), parts * size), :]
        ref = (wb, wc, wu, None, wgu)[t]
        size = depth // 2
        return ref.at[pl.ds(pl.multiple_of(index * depth + first * size, 16), parts * size), :]

    def remote(src, dst, send, recv, device):
        return pltpu.make_async_remote_copy(
            src_ref=src, dst_ref=dst, send_sem=send, recv_sem=recv, device_id=device, device_id_type=MESH
        )


    def local(t):
        return pltpu.make_async_copy(source(t, y), slot(t, fs), load_sem.at[t])

    def y_copy(t, index):
        return remote(source(t, 1 - y), slot(t, index), y_send.at[t], y_recv.at[t], mate)

    def z_own(t, rr, side):
        index = line(rr, z)
        src = source(t, y, rep) if rr == 0 else slot(t, index, rep)
        return remote(
            src, slot(t, index, rep), zown_send.at[t, rr, (side + 1) // 2], z_recv.at[t, rr, z], along(z + side)
        )

    def z_fwd(t, rr, position, target):
        place = slot(t, line(rr, position), rep)
        return remote(place, place, zfwd_send.at[t, rr, position], z_recv.at[t, rr, position], along(target))

    def x_copy(t, rr, position, piece):
        place = slot(t, line(rr, position), piece)
        return remote(place, place, x_send.at[t, rr, position], x_recv.at[t, rr, position], twin)

    def z_each(group, rr, act):
        for side in (-1, 1):

            @pl.when(jnp.logical_and(z + side >= 0, z + side < n_z))
            def _():
                for t in group:
                    act(z_own(t, rr, side))

    def start_own(group, rr):
        if rr == 1:
            for t in group:
                y_copy(t, line(1, z)).wait_recv()
        z_each(group, rr, lambda copy: copy.start())

    def relay(group, rr, k):
        position = kth(k)
        onward = z + jnp.where(position < z, 1, -1)
        for t in group:
            z_fwd(t, rr, position, z).wait_recv()

            @pl.when(jnp.logical_and(onward >= 0, onward < n_z))
            def _(t=t):
                z_fwd(t, rr, position, onward).start()

            x_copy(t, rr, position, rep).start()

    def x_wait(group, pairs):
        for rr, k in pairs:
            for t in group:
                x_copy(t, rr, kth(k), 1 - rep).wait_recv()

    everything = [(rr, k) for rr in range(2) for k in range(1, n_z)]


    def half_rows(which, first=0, count=None):
        return pl.ds(pl.multiple_of(which * rows + first, 16), rows if count is None else count)

    def core_copy(src, dst, sems, place):
        return remote(src, dst, sems[0].at[place], sems[1].at[place], core)

    def mate_copy(src, dst, sems, place):
        return remote(src, dst, sems[0].at[place], sems[1].at[place], mate)

    one, mix, mid, two = (one_send, one_recv), (mix_send, mix_recv), (mid_send, mid_recv), (two_send, two_recv)
    mine, other = half_rows(tp), half_rows(1 - tp)


    barrier = pltpu.get_barrier_semaphore()
    for device in (core, mate, twin):
        pl.semaphore_signal(barrier, inc=1, device_id=device, device_id_type=MESH)
    neighbours = 3
    for side in (-1, 1):
        inside = jnp.logical_and(z + side >= 0, z + side < n_z)
        neighbours += inside.astype(jnp.int32)

        @pl.when(inside)
        def _(side=side):
            pl.semaphore_signal(barrier, inc=1, device_id=along(z + side), device_id_type=MESH)

    load = pltpu.make_async_copy(tok_hbm, tok, load_sem.at[6])
    load.start()
    pl.semaphore_wait(barrier, neighbours)
    for t in INPUT:
        y_copy(t, fs).start()
        z_each((t,), 0, lambda copy: copy.start())
    for t in INPUT + OUT + GU + DN:
        local(t).start()
    load.wait()

    @pl.loop(0, rows // STRIP)
    def _(i):
        at = pl.ds(pl.multiple_of(i * STRIP, STRIP), STRIP)
        values = f32(tok[at, :])
        factor = lax.rsqrt(jnp.mean(values * values, axis=-1, keepdims=True) + 1e-06)
        normed[0, pl.ds(pl.multiple_of(tp * rows + i * STRIP, STRIP), STRIP), :] = (
            values * factor * gain_one[...]
        ).astype(jnp.bfloat16)

    one_core = core_copy(normed.at[0, mine, :], normed.at[0, mine, :], one, 0)
    one_mate = mate_copy(normed.at[0, mine, :], normed.at[1, mine, :], one, 1)
    one_pass = core_copy(normed.at[1, mine, :], normed.at[1, mine, :], one, 2)
    one_core.start()
    one_mate.start()
    for t in OUT + GU + DN:
        y_copy(t, fs).start()


    for k in range(1, n_z):
        relay(INPUT, 0, k)
    start_own(INPUT, 1)
    for k in range(1, n_z):
        relay(INPUT, 1, k)
    one_mate.wait_recv()
    one_pass.start()
    start_own(OUT, 0)
    start_own(OUT, 1)
    for t in INPUT:
        local(t).wait()
    x_wait(INPUT, everything)
    core_copy(normed.at[0, other, :], normed.at[0, other, :], one, 0).wait_recv()
    core_copy(normed.at[1, other, :], normed.at[1, other, :], one, 2).wait_recv()

    my_taps = pl.ds(pl.multiple_of((tp * 2 + y) * channels, 128), channels)

    def project_in(seq, half):
        at = pl.ds(half * rows, rows)
        part_rows = normed[seq, at, :]
        mixed = f32(mxu(part_rows, wc[...]).astype(jnp.bfloat16)) * f32(mxu(part_rows, wu[...]).astype(jnp.bfloat16))
        row = lax.broadcasted_iota(jnp.int32, mixed.shape, 0)
        before = [jnp.zeros((1, channels), jnp.float32)] * 2 if half == 0 else [tail[0:1, :], tail[1:2, :]]
        back_one = jnp.where(row == 0, before[1], pltpu.roll(mixed, 1, 0))
        back_two = jnp.where(row == 0, before[0], jnp.where(row == 1, before[1], pltpu.roll(mixed, 2, 0)))
        if half == 0:
            tail[0:2, :] = mixed[rows - 2 : rows, :]
        convolved = (
            taps[0:1, my_taps] * back_two + taps[1:2, my_taps] * back_one + taps[2:3, my_taps] * mixed
        )
        b_proj = f32(mxu(part_rows, wb[...]).astype(jnp.bfloat16))
        gated[seq, at, :] = (b_proj * convolved).astype(jnp.bfloat16)

    turns = list(everything)
    for seq in (1, 0):
        for half in range(2):
            project_in(seq, half)
            for rr, k in turns[:2]:
                relay(OUT, rr, k)
            turns = turns[2:]
    for rr, k in turns:
        relay(OUT, rr, k)
    start_own(GU, 0)
    start_own(GU, 1)
    local(3).wait()
    x_wait(OUT, everything)

    def project_out(seq, at):
        left = gated[seq, at, :]
        for index in range(n_fs):
            part[seq, at, index * width : (index + 1) * width] = mxu(left, wo[index]).astype(jnp.bfloat16)

    mix_core = [core_copy(part.at[s, other, :], theirs.at[s], mix, s) for s in range(2)]
    project_out(1, other)
    mix_core[1].start()
    project_out(1, mine)
    mix_core[1].wait_recv()
    halves = [pl.ds(i * sub, sub) for i in range(2)]
    mix_mate = [mate_copy(outgo.at[at, :], income.at[at, :], mix, 2 + i) for i, at in enumerate(halves)]
    strips = sub // STRIP
    for i in range(2):

        @pl.loop(0, strips)
        def _(j, i=i):
            first = i * sub + j * STRIP
            at = pl.ds(pl.multiple_of(first, STRIP), STRIP)
            outgo[at, :] = (f32(part[1, half_rows(tp, first, STRIP), :]) + f32(theirs[1, at, :])).astype(jnp.bfloat16)

        mix_mate[i].start()
    relay(GU, 0, 1)
    project_out(0, other)
    mix_core[0].start()
    project_out(0, mine)
    mix_core[0].wait_recv()
    relay(GU, 0, 2)
    relay(GU, 0, 3) if n_z > 3 else None

    def piece(which, i):
        return half_rows(which, i * sub, sub)

    def mid_core(which, i):
        return core_copy(normed_two.at[0, piece(which, i), :], normed_two.at[0, piece(which, i), :], mid, i)

    def mid_mate(i):
        return mate_copy(normed_two.at[0, piece(tp, i), :], normed_two.at[1, piece(tp, i), :], mid, 2 + i)

    def mid_pass(which, i):
        return core_copy(normed_two.at[1, piece(which, i), :], normed_two.at[1, piece(which, i), :], mid, 4 + i)

    for i in range(2):
        mix_mate[i].wait_recv()

        @pl.loop(0, strips)
        def _(j, i=i):
            first = i * sub + j * STRIP
            at = pl.ds(pl.multiple_of(first, STRIP), STRIP)
            here = half_rows(tp, first, STRIP)
            values = f32(tok[at, :]) + ((f32(part[0, here, :]) + f32(theirs[0, at, :])) + f32(income[at, :]))
            res[at, :] = values
            factor = lax.rsqrt(jnp.mean(values * values, axis=-1, keepdims=True) + 1e-06)
            normed_two[0, here, :] = (values * factor * gain_two[...]).astype(jnp.bfloat16)

        mid_mate(i).start()
        mid_core(tp, i).start()
        if i == 0:
            relay(GU, 1, 1)
    for k in range(2, n_z):
        relay(GU, 1, k)
    start_own(DN, 0)
    start_own(DN, 1)


    def feed(seq, at):
        both = mxu(normed_two[seq, at, :], wgu[...])
        gate, up = both[:, :units], both[:, units:]
        hidden[seq, at, :] = (gate / (1.0 + jnp.exp(-gate)) * up).astype(jnp.bfloat16)

    mid_mate(0).wait_recv()
    mid_pass(tp, 0).start()
    local(4).wait()
    x_wait(GU, everything)
    feed(0, mine)
    relay(DN, 0, 1)
    mid_core(1 - tp, 0).wait_recv()
    mid_core(1 - tp, 1).wait_recv()
    feed(0, other)
    relay(DN, 0, 2)
    feed(1, piece(tp, 0))
    mid_pass(1 - tp, 0).wait_recv()
    feed(1, piece(1 - tp, 0))
    for k in range(3, n_z):
        relay(DN, 0, k)
    mid_mate(1).wait_recv()
    mid_pass(tp, 1).start()
    relay(DN, 1, 1)
    feed(1, piece(tp, 1))
    mid_pass(1 - tp, 1).wait_recv()
    feed(1, piece(1 - tp, 1))
    local(5).wait()

    def two_core(index):
        return core_copy(part_two.at[index, :, other, :], theirs_two.at[index], two, index)

    def two_mate(index):
        return mate_copy(outgo_two.at[index], income_two.at[index], two, n_fs + index)

    def down(index):
        right = wd[index]
        for seq in range(2):
            for half in range(2):
                at = pl.ds(half * rows, rows)
                part_two[index, seq, at, :] = mxu(hidden[seq, at, :], right).astype(jnp.bfloat16)
        two_core(index).start()

    def add_cores(index):
        two_core(index).wait_recv()
        outgo_two[index] = (f32(part_two[index, 1, mine, :]) + f32(theirs_two[index, 1])).astype(jnp.bfloat16)
        two_mate(index).start()

    order = [line(rr, z if k == 0 else kth(k)) for k in range(n_z) for rr in range(2)]
    for place, index in enumerate(order):
        k, rr = place // 2, place % 2
        if k > 0:
            x_wait(DN, [(rr, k)])
        down(index)
        if place > 0:
            add_cores(order[place - 1])
        if 1 <= place < n_z - 1:
            relay(DN, 1, place + 1)
    add_cores(order[-1])
    stores = []
    for place, index in enumerate(order):
        two_mate(index).wait_recv()
        cols = pl.ds(pl.multiple_of(index * width, 128), width)
        total = (f32(part_two[index, 0, mine, :]) + f32(theirs_two[index, 0])) + f32(income_two[index])
        final[:, cols] = (res[:, cols] + 0.5 * total).astype(jnp.bfloat16)
        stores.append(pltpu.make_async_copy(final.at[:, cols], out_hbm.at[:, cols], store_sem.at[place]))
        stores[-1].start()


    for t in INPUT + OUT + GU + DN:
        y_copy(t, fs).wait_send()
        for rr in range(2):
            z_each((t,), rr, lambda copy: copy.wait_send())
            for k in range(1, n_z):
                position = kth(k)
                onward = z + jnp.where(position < z, 1, -1)
                x_copy(t, rr, position, rep).wait_send()

                @pl.when(jnp.logical_and(onward >= 0, onward < n_z))
                def _(t=t, rr=rr, position=position, onward=onward):
                    z_fwd(t, rr, position, onward).wait_send()

    sent = [one_core, one_mate, one_pass, *mix_core, *mix_mate]
    sent += [make for i in range(2) for make in (mid_core(tp, i), mid_mate(i), mid_pass(tp, i))]
    sent += [make for index in order for make in (two_core(index), two_mate(index))]
    for copy in sent:
        copy.wait_send()
    for copy in stores:
        copy.wait()


def block(
    n_fs, tokens, mix_gain, w_bgate, w_cgate, w_value, conv_taps, w_mixout, mlp_gain, w_gate, w_up, w_down
):
    rows, dim = tokens.shape
    depth, channels = w_bgate.shape[0], w_bgate.shape[1] // 2
    units = w_gate.shape[1] // 2
    width = w_mixout.shape[1]
    n_z = n_fs // 2
    bf16 = jnp.bfloat16
    w_gu = jnp.concatenate(
        [w[:, h * units : (h + 1) * units] for h in range(2) for w in (w_gate, w_up)], axis=1
    )
    hbm = pl.BlockSpec(memory_space=pl.ANY)
    vmem = pl.BlockSpec(memory_space=pltpu.VMEM)
    dma = pltpu.SemaphoreType.DMA
    return pl.pallas_call(
        functools.partial(kernel, n_z),
        out_shape=jax.ShapeDtypeStruct(tokens.shape, tokens.dtype),
        in_specs=[hbm, vmem, hbm, hbm, hbm, vmem, hbm, vmem, hbm, hbm],
        out_specs=hbm,
        scratch_shapes=[
            *[pltpu.VMEM((n_fs * depth, channels), bf16)] * 3,
            pltpu.VMEM((n_fs, w_mixout.shape[0] // 2, width), bf16),
            pltpu.VMEM((n_fs * depth, 2 * units), bf16),
            pltpu.VMEM((n_fs, w_down.shape[0] // 2, width), bf16),
            pltpu.VMEM((rows, dim), bf16),
            pltpu.VMEM((2, 2 * rows, dim), bf16),
            pltpu.VMEM((2, 2 * rows, channels), bf16),
            pltpu.VMEM((2, 2 * rows, dim), bf16),
            pltpu.VMEM((2, rows, dim), bf16),
            pltpu.VMEM((rows, dim), bf16),
            pltpu.VMEM((rows, dim), bf16),
            pltpu.VMEM((rows, dim), jnp.float32),
            pltpu.VMEM((2, 2 * rows, dim), bf16),
            pltpu.VMEM((2, 2 * rows, units), bf16),
            pltpu.VMEM((n_fs, 2, 2 * rows, width), bf16),
            pltpu.VMEM((n_fs, 2, rows, width), bf16),
            pltpu.VMEM((n_fs, rows, width), bf16),
            pltpu.VMEM((n_fs, rows, width), bf16),
            pltpu.VMEM((rows, dim), bf16),
            pltpu.VMEM((8, channels), jnp.float32),
            dma((7,)),
            dma((6,)),
            dma((6,)),
            dma((6, 2, 2)),
            *[dma((6, 2, n_z))] * 4,
            *[dma((3,))] * 2,
            *[dma((4,))] * 2,
            *[dma((6,))] * 2,
            *[dma((2 * n_fs,))] * 2,
            dma((n_fs,)),
        ],
        compiler_params=pltpu.CompilerParams(
            collective_id=0, has_side_effects=True, vmem_limit_bytes=66_900_000
        ),
    )(
        tokens, mix_gain[None], w_bgate, w_cgate, w_value, conv_taps, w_mixout, mlp_gain[None], w_gu, w_down
    )


SPECS = (
    P(("rep", "fs", "tp"), None),
    P(),
    P("fs", "tp"),
    P("fs", "tp"),
    P("fs", "tp"),
    P(),
    P("tp", "fs"),
    P(),
    P("fs", "tp"),
    P("fs", "tp"),
    P("tp", "fs"),
)


def permuted(mesh):
    return jax.shard_map(
        build(mesh.shape["fs"]),
        mesh=mesh,
        in_specs=SPECS,
        out_specs=P(("rep", "fs", "tp"), None),
        check_vma=False,
    )


def fused(mesh):
    return jax.shard_map(
        functools.partial(block, mesh.shape["fs"]),
        mesh=mesh,
        in_specs=SPECS,
        out_specs=P(("rep", "fs", "tp"), None),
        check_vma=False,
    )


def solution(mesh):
    n_fs, n_rep, n_tp = (mesh.shape[name] for name in ("fs", "rep", "tp"))

    def step(*operands):
        tokens, w_down = operands[0], operands[-1]
        rows = tokens.shape[0] // (n_rep * n_fs * n_tp)
        width = tokens.shape[1] // n_fs
        units = w_down.shape[0] // n_tp
        aligned = (
            (n_rep, n_tp, n_fs % 2) == (2, 2, 0)
            and (rows % (2 * STRIP), width % LANES, units % (4 * STRIP), units % LANES) == (0, 0, 0, 0)
            and tokens.shape[1] % (4 * LANES) == 0
        )
        return (fused if aligned else permuted)(mesh)(*operands)

    return step
```

profile of v0, /device:TPU:0, one launch (start us, length us, event | category | flops | bytes accessed | tf_op | source)
XLA Modules:
  0.0 198.2 jit_solution(13367684402041535842)
XLA Ops:
  0.0 1.8 fusion
  1.8 2.3 %concatenate.3.wgu_hbm = bf16[256,2816]{1,0:T(8,128)(2,1)} concatenate(bf16[256,704]{1,0:T(8,128)(2,1)S(1)} %get-tuple-element.9, bf16[256,704]{1,0:T(8,128)(2,1)S(1)} %get-tuple-element.6, bf16[256,704]{1,0:T(8,128)(2,1)S(1)} %get-tuple-element.10, bf16[256,704]{1,0:T(8,128)(2,1)S(1)} %get-tuple-element.5), dimensions={1} | concatenate | bytes 2883584 | tf_op jit(solution)/shard_map/concatenate | solution.py:556
  4.1 191.6 %shard_map.109 = bf16[320,2048]{1,0:T(8,128)(2,1)} custom-call(bf16[320,2048]{1,0:T(8,128)(2,1)} %tok_hbm.1, f32[1,2048]{1,0:T(1,128)} %bitcast.2, bf16[256,1024]{1,0:T(8,128)(2,1)} %wb_hbm.1, bf16[256,1024]{1,0:T(8,128)(2,1)} %wc_hbm.1, bf16[256,1024]{1,0:T(8,128)(2,1)} %wu_hbm.1, f32[3,2048]{1,0:T(4,128)} %taps.1, bf16[1024,256]{1,0:T(8,128)(2,1)} %wo_hbm.1, ...), custom_call_target="tpu_custom_call" | custom-call | tf_op jit(solution)/shard_map/pallas_call | solution.py:562
  195.6 2.5 %copy.13 = bf16[320,2048]{1,0:T(8,128)(2,1)} copy(bf16[320,2048]{1,0:T(8,128)(2,1)} %shard_map.109) | data formatting | bytes 2621440
where the time goes:
time: 198 us
  Pallas kernels  192 us (97%)
  local copies, waits for them, and re-layouts  6.58 us (3%)
    pallas_call x1, Pallas kernels, block(): pl.pallas_call(functools.partial(kernel, n_z), out_shape=jax.ShapeDtypeSt...  192 us

commit v1 on v0

v1 whole, which is shorter than its diff:
```python
import functools

import jax
import jax.numpy as jnp
from jax import lax
from jax.experimental import pallas as pl
from jax.experimental.pallas import tpu as pltpu
from jax.sharding import PartitionSpec as P


def rms_scale(matrix, gain):
    values = matrix.astype(jnp.float32)
    factor = lax.rsqrt(jnp.mean(values * values, axis=-1, keepdims=True) + 1e-06)
    return values * factor * gain


def causal_taps(mixed, filters):
    length = mixed.shape[-2]
    padded = jnp.pad(mixed, [(2, 0), (0, 0)])
    return (
        filters[0] * padded[0:length]
        + filters[1] * padded[1 : length + 1]
        + filters[2] * padded[2 : length + 2]
    )


def swap(array, axis):
    return lax.ppermute(array, axis, [(0, 1), (1, 0)])


def half(array, axis, part):
    size = array.shape[axis] // 2
    return lax.dynamic_slice_in_dim(array, part * size, size, axis)


def build(n_fs):
    ring = [(i, (i + 2) % n_fs) for i in range(n_fs)]
    pair = [(i, i ^ 1) for i in range(n_fs)]
    steps = n_fs // 2

    def ring_first(block):
        blocks = []
        for step in range(steps):
            blocks += [block, lax.ppermute(block, "fs", pair)]
            if step < steps - 1:
                block = lax.ppermute(block, "fs", ring)
        return blocks

    def pair_first(block):
        mate = lax.ppermute(block, "fs", pair)
        blocks = []
        for step in range(steps):
            blocks += [block, mate]
            if step < steps - 1:
                block = lax.ppermute(block, "fs", ring)
                mate = lax.ppermute(mate, "fs", ring)
        return blocks

    def on_device(
        tokens, mix_gain, w_bgate, w_cgate, w_value, conv_taps, w_mixout, mlp_gain, w_gate, w_up, w_down
    ):
        rep, fs, tp = (lax.axis_index(name) for name in ("rep", "fs", "tp"))
        width = tokens.shape[1] // n_fs

        def arrival_order(array):
            order = [((fs ^ j) - 2 * s + n_fs) % n_fs for s in range(steps) for j in range(2)]
            return jnp.concatenate(
                [lax.dynamic_slice_in_dim(array, k * width, width, array.ndim - 1) for k in order],
                axis=-1,
            )

        def global_order(array):
            places = []
            for k in range(n_fs):
                j = (fs ^ k) & 1
                places.append((((fs ^ j) - k + n_fs) % n_fs) + j)
            return jnp.concatenate(
                [lax.dynamic_slice_in_dim(array, k * width, width, array.ndim - 1) for k in places],
                axis=-1,
            )

        def sequence(rows):
            other = swap(rows, "tp")
            return jnp.concatenate(
                [jnp.where(tp == 0, rows, other), jnp.where(tp == 0, other, rows)], axis=0
            )

        def both_sequences(rows):
            away = swap(rows, "rep")
            return sequence(rows), sequence(away)

        def chip_sum(partial):
            other = swap(half(partial, 0, 1 - tp), "tp")
            return half(partial, 0, tp).astype(jnp.float32) + other.astype(jnp.float32)

        def project_out(mine, theirs, blocks, group):
            sums = []
            for start in range(0, len(blocks), group):
                weight = jnp.concatenate(blocks[start : start + group], axis=1)
                outs = []
                for rows in (theirs, mine):
                    outs.append(
                        jnp.dot(rows, weight, preferred_element_type=jnp.float32).astype(
                            jnp.bfloat16
                        )
                    )
                away = swap(chip_sum(outs[0]).astype(jnp.bfloat16), "rep")
                sums.append(chip_sum(outs[1]) + away.astype(jnp.float32))
            return jnp.concatenate(sums, axis=1)

        w_in = jnp.concatenate([half(w, 1, rep) for w in (w_bgate, w_cgate, w_value)], axis=1)
        w_gu = jnp.concatenate([half(w, 1, rep) for w in (w_gate, w_up)], axis=1)
        in_blocks = ring_first(w_in)
        out_blocks = ring_first(half(w_mixout, 0, rep))
        upper, lower = jnp.split(w_gu, 2, axis=0)
        gu_blocks = [part for both in zip(pair_first(upper), ring_first(lower)) for part in both]
        down_blocks = ring_first(half(w_down, 0, rep))

        channels = w_in.shape[1] // 3
        taps = lax.dynamic_slice_in_dim(conv_taps, (tp * 2 + rep) * channels, channels, 1)
        local = arrival_order(tokens)

        def mix(normed, weight):
            projected = jnp.dot(normed, weight, preferred_element_type=jnp.float32).astype(
                jnp.bfloat16
            )
            b_proj, c_proj, u_proj = (
                projected[:, k * channels : (k + 1) * channels].astype(jnp.float32)
                for k in range(3)
            )
            return (b_proj * causal_taps(c_proj * u_proj, taps)).astype(jnp.bfloat16)

        mine, theirs = both_sequences(rms_scale(local, arrival_order(mix_gain)).astype(jnp.bfloat16))
        weight = jnp.concatenate(in_blocks, axis=0)
        theirs, mine = mix(theirs, weight), mix(mine, weight)
        mixed = project_out(mine, theirs, out_blocks, 2)
        residual = local.astype(jnp.float32) + mixed

        units = w_gu.shape[1] // 2

        def feed(normed, weight):
            both = jnp.dot(normed, weight, preferred_element_type=jnp.float32)
            return (jax.nn.silu(both[:, :units]) * both[:, units:]).astype(jnp.bfloat16)

        mine, theirs = both_sequences(rms_scale(residual, arrival_order(mlp_gain)).astype(jnp.bfloat16))
        weight = jnp.concatenate(gu_blocks, axis=0)
        theirs, mine = feed(theirs, weight), feed(mine, weight)
        down = project_out(mine, theirs, down_blocks, 2)
        return global_order((residual + 0.5 * down).astype(jnp.bfloat16))

    return on_device


MESH = pl.DeviceIdType.MESH
STRIP = 16
LANES = 128
C, U, B, OUT, GA, GB, DN = TYPES = range(7)
SHARED = (DN,)


def f32(value):
    return value.astype(jnp.float32)


def mxu(left, right):
    return jnp.dot(left, right, preferred_element_type=jnp.float32)


def kernel(
    n_z,
    tok_hbm, gain_one, wb_hbm, wc_hbm, wu_hbm, taps, wo_hbm, gain_two, wg_hbm, wup_hbm, wd_hbm,
    final,
    wb, wc, wu, wo, wgu, wd,
    raw_gate, raw_up, away,
    tok, normed, convolved, gated, part, theirs, outgo, income, res, normed_two, hidden,
    part_two, theirs_two, outgo_two, income_two,
    tail,
    load_sem, y_send, y_recv, zown_send, zfwd_send, z_recv, x_send, x_recv,
    one_send, one_recv, mix_send, mix_recv, mid_send, mid_recv, two_send, two_recv,
):
    rep, fs, tp = (lax.axis_index(name) for name in ("rep", "fs", "tp"))
    z, y = lax.div(fs, 2), lax.rem(fs, 2)
    rows, _ = tok.shape
    sub = rows // 2
    depth = wb_hbm.shape[0]
    channels = wb.shape[1]
    pair_units = wgu.shape[1]
    units = pair_units // 2
    width = wo.shape[2]
    n_fs = 2 * n_z
    core = (rep, fs, 1 - tp)
    mate = (rep, z * 2 + 1 - y, tp)
    twin = (1 - rep, fs, tp)

    def along(position):
        return (rep, position * 2 + y, tp)

    def kth(k):
        near = jnp.minimum(z, n_z - 1 - z)
        longer = jnp.where(z < n_z - 1 - z, 1, -1)
        both = z + longer * (((k + 1) // 2) * (1 if k % 2 == 1 else -1))
        return jnp.where(k <= 2 * near, both, z + longer * (k - near))

    def line(rr, position):
        return position * 2 + (y if rr == 0 else 1 - y)

    def rows_of(t, piece, base):
        if t in (OUT, DN):
            size = (wo, wd)[t == DN].shape[1] // 2
        else:
            size = depth // (4 if t in (GA, GB) else 2)
        first = base + (2 * size if t == GB else 0)
        if piece is None:
            return pl.ds(pl.multiple_of(first, 16), 2 * size)
        return pl.ds(pl.multiple_of(first + piece * size, 16), size)

    def source(t, half, piece=None):
        if t in (OUT, DN):
            ref = (wo_hbm, wd_hbm)[t == DN]
            return ref.at[rows_of(t, piece, half * (ref.shape[0] // 2)), :]
        ref = (wc_hbm, wu_hbm, wb_hbm)[t]
        return ref.at[rows_of(t, piece, 0), pl.ds(pl.multiple_of(half * channels, 128), channels)]

    def slot(t, index, piece=None):
        if t in (OUT, DN):
            return (wo, wd)[t == DN].at[index, rows_of(t, piece, 0), :]
        return (wc, wu, wb, None, wgu, wgu)[t].at[rows_of(t, piece, index * depth), :]

    def remote(src, dst, send, recv, device):
        return pltpu.make_async_remote_copy(
            src_ref=src, dst_ref=dst, send_sem=send, recv_sem=recv, device_id=device, device_id_type=MESH
        )


    def local(t):
        return pltpu.make_async_copy(source(t, y), slot(t, fs), load_sem.at[t])

    def y_copy(t, index):
        piece = rep if t in SHARED else None
        src = away.at[rows_of(t, piece, 0), :] if t in (GA, GB) else source(t, 1 - y, piece)
        return remote(src, slot(t, index, piece), y_send.at[t], y_recv.at[t], mate)

    def z_own(t, rr, side):
        index = line(rr, z)
        src = slot(t, index, rep) if rr == 1 or t in (GA, GB) else source(t, y, rep)
        return remote(
            src, slot(t, index, rep), zown_send.at[t, rr, (side + 1) // 2], z_recv.at[t, rr, z], along(z + side)
        )

    def z_fwd(t, rr, position, target):
        place = slot(t, line(rr, position), rep)
        return remote(place, place, zfwd_send.at[t, rr, position], z_recv.at[t, rr, position], along(target))

    def x_copy(t, rr, position, piece):
        place = slot(t, line(rr, position), piece)
        return remote(place, place, x_send.at[t, rr, position], x_recv.at[t, rr, position], twin)

    def z_each(t, rr, act):
        for side in (-1, 1):

            @pl.when(jnp.logical_and(z + side >= 0, z + side < n_z))
            def _():
                act(z_own(t, rr, side))

    def start_own(t, rr):
        if rr == 1:
            y_copy(t, line(1, z)).wait_recv()
            if t in SHARED:
                x_copy(t, 1, z, rep).start()
        z_each(t, rr, lambda copy: copy.start())

    def relay(t, rr, k):
        position = kth(k)
        onward = z + jnp.where(position < z, 1, -1)
        z_fwd(t, rr, position, z).wait_recv()

        @pl.when(jnp.logical_and(onward >= 0, onward < n_z))
        def _():
            z_fwd(t, rr, position, onward).start()

        x_copy(t, rr, position, rep).start()

    def x_wait(t, pairs):
        for rr, k in pairs:
            x_copy(t, rr, kth(k), 1 - rep).wait_recv()

    def x_all(t):
        x_wait(t, [(rr, k) for rr in range(2) for k in range(1, n_z)] + [(1, 0)] * (t in SHARED))


    def half_rows(which, first=0, count=None):
        return pl.ds(pl.multiple_of(which * rows + first, 16), rows if count is None else count)

    def core_copy(src, dst, sems, place):
        return remote(src, dst, sems[0].at[place], sems[1].at[place], core)

    def mate_copy(src, dst, sems, place):
        return remote(src, dst, sems[0].at[place], sems[1].at[place], mate)

    one, mix, mid, two = (one_send, one_recv), (mix_send, mix_recv), (mid_send, mid_recv), (two_send, two_recv)
    mine, other = half_rows(tp), half_rows(1 - tp)


    barrier = pltpu.get_barrier_semaphore()
    for device in (core, mate, twin):
        pl.semaphore_signal(barrier, inc=1, device_id=device, device_id_type=MESH)
    neighbours = 3
    for side in (-1, 1):
        inside = jnp.logical_and(z + side >= 0, z + side < n_z)
        neighbours += inside.astype(jnp.int32)

        @pl.when(inside)
        def _(side=side):
            pl.semaphore_signal(barrier, inc=1, device_id=along(z + side), device_id_type=MESH)

    raw = [
        pltpu.make_async_copy(src, dst, load_sem.at[place])
        for src, dst, place in ((tok_hbm, tok, GA), (wg_hbm, raw_gate, GB), (wup_hbm, raw_up, DN + 1))
    ]
    raw[0].start()
    pl.semaphore_wait(barrier, neighbours)
    for t in (C, U, B):
        y_copy(t, fs).start()
    for t in (C, U, B):
        start_own(t, 0)
    for copy in raw[1:]:
        copy.start()
    for t in (C, U, B, OUT, DN):
        local(t).start()
    raw[0].wait()

    @pl.loop(0, rows // STRIP)
    def _(i):
        at = pl.ds(pl.multiple_of(i * STRIP, STRIP), STRIP)
        values = f32(tok[at, :])
        factor = lax.rsqrt(jnp.mean(values * values, axis=-1, keepdims=True) + 1e-06)
        normed[0, pl.ds(pl.multiple_of(tp * rows + i * STRIP, STRIP), STRIP), :] = (
            values * factor * gain_one[...]
        ).astype(jnp.bfloat16)

    one_core = core_copy(normed.at[0, mine, :], normed.at[0, mine, :], one, 0)
    one_mate = mate_copy(normed.at[0, mine, :], normed.at[1, mine, :], one, 1)
    one_pass = core_copy(normed.at[1, mine, :], normed.at[1, mine, :], one, 2)
    y_copy(OUT, fs).start()
    one_core.start()
    one_mate.start()

    def relays(types, rr, k):
        for t in types:
            relay(t, rr, k)

    three = (C, U, B)
    relays(three, 0, 1)
    start_own(C, 1)
    for copy in raw[1:]:
        copy.wait()

    @pl.loop(0, depth // STRIP)
    def _(i):
        at = pl.ds(pl.multiple_of(i * STRIP, STRIP), STRIP)
        here = pl.ds(pl.multiple_of(fs * depth + i * STRIP, STRIP), STRIP)
        gate, up = f32(raw_gate[at, :]), f32(raw_up[at, :])
        for half in range(2):
            cut = slice(half * units, (half + 1) * units)
            both = jnp.concatenate([gate[:, cut], up[:, cut]], axis=1).astype(jnp.bfloat16)

            @pl.when(y == half)
            def _(both=both):
                wgu[here, :] = both

            @pl.when(y != half)
            def _(both=both):
                away[at, :] = both

    for t in (GA, GB, DN):
        y_copy(t, fs).start()


    my_taps = pl.ds(pl.multiple_of((tp * 2 + y) * channels, 128), channels)

    def convolve(seq, half):
        at = pl.ds(half * rows, rows)
        left = normed[seq, at, :]
        mixed = f32(mxu(left, wc[...]).astype(jnp.bfloat16)) * f32(mxu(left, wu[...]).astype(jnp.bfloat16))
        row = lax.broadcasted_iota(jnp.int32, mixed.shape, 0)
        before = [jnp.zeros((1, channels), jnp.float32)] * 2 if half == 0 else [tail[0:1, :], tail[1:2, :]]
        back_one = jnp.where(row == 0, before[1], pltpu.roll(mixed, 1, 0))
        back_two = jnp.where(row == 0, before[0], jnp.where(row == 1, before[1], pltpu.roll(mixed, 2, 0)))
        if half == 0:
            tail[0:2, :] = mixed[rows - 2 : rows, :]
        convolved[seq, at, :] = (
            taps[0:1, my_taps] * back_two + taps[1:2, my_taps] * back_one + taps[2:3, my_taps] * mixed
        )

    def gate_out(seq, half):
        at = pl.ds(half * rows, rows)
        b_proj = f32(mxu(normed[seq, at, :], wb[...]).astype(jnp.bfloat16))
        gated[seq, at, :] = (b_proj * convolved[seq, at, :]).astype(jnp.bfloat16)

    arrivals = sorted((max(k, 2), rr, k) for rr in range(2) for k in range(1, n_z))
    for place, (_, rr, k) in enumerate(arrivals[1:]):
        if place == len(arrivals) - 3:
            start_own(OUT, 0)
        relays(three, rr, k)
        if place == 0:
            start_own(U, 1)
            start_own(B, 1)
    start_own(OUT, 1)
    relay(OUT, 0, 1)
    relay(OUT, 1, 1)
    one_mate.wait_recv()
    one_pass.start()
    for t in (C, U):
        local(t).wait()
        x_all(t)
    core_copy(normed.at[1, other, :], normed.at[1, other, :], one, 2).wait_recv()

    def mix_core(index):
        return core_copy(part.at[index, 1, other, :], theirs.at[index, 1], mix, index * 3)

    def mix_mate(index):
        return mate_copy(outgo.at[index], income.at[index], mix, index * 3 + 1)

    def mix_own(index):
        return core_copy(part.at[index, 0, other, :], theirs.at[index, 0], mix, index * 3 + 2)

    def project_out(index, seq):
        right = wo[index]
        for at in (other, mine):
            part[index, seq, at, :] = mxu(gated[seq, at, :], right).astype(jnp.bfloat16)
            if at is other:
                (mix_own, mix_core)[seq](index).start()

    def send_sum(index):
        mix_core(index).wait_recv()
        outgo[index] = (f32(part[index, 1, mine, :]) + f32(theirs[index, 1])).astype(jnp.bfloat16)
        mix_mate(index).start()

    order = [line(rr, kth(k)) for k in range(n_z) for rr in range(2)]

    convolve(1, 0)
    relay(OUT, 0, 2)
    convolve(1, 1)
    relay(OUT, 1, 2)
    local(B).wait()
    x_all(B)
    gate_out(1, 0)
    gate_out(1, 1)
    local(OUT).wait()
    project_out(order[0], 1)
    project_out(order[1], 1)
    send_sum(order[0])
    send_sum(order[1])
    for k in range(3, n_z):
        relay(OUT, 0, k)
        relay(OUT, 1, k)
    for t in (GA, GB):
        for rr in range(2):
            start_own(t, rr)
    core_copy(normed.at[0, other, :], normed.at[0, other, :], one, 0).wait_recv()
    gu = [(t, rr) for t in (GA, GB) for rr in range(2)]
    todo = [(*pair, k) for k in range(1, n_z) for pair in gu]
    todo.reverse()
    for place in range(2, 2 * n_z):
        x_wait(OUT, [(place % 2, place // 2)])
        project_out(order[place], 1)
        if place > 2:
            send_sum(order[place - 1])
        if place % 2 == 1:
            relay(*todo.pop())
    send_sum(order[-1])
    convolve(0, 0)
    relay(*todo.pop())
    convolve(0, 1)
    gate_out(0, 0)
    gate_out(0, 1)
    relay(*todo.pop())
    for index in order:
        project_out(index, 0)

    def add_up(index):
        mix_own(index).wait_recv()
        mix_mate(index).wait_recv()
        cols = pl.ds(pl.multiple_of(index * width, 128), width)
        res[:, cols] = f32(tok[:, cols]) + (
            (f32(part[index, 0, mine, :]) + f32(theirs[index, 0])) + f32(income[index])
        )

    relay(*todo.pop())
    relay(*todo.pop())
    for index in order:
        add_up(index)

    halves = [pl.ds(i * sub, sub) for i in range(2)]
    strips = sub // STRIP

    def piece(which, i):
        return half_rows(which, i * sub, sub)

    def mid_core(which, i):
        return core_copy(normed_two.at[0, piece(which, i), :], normed_two.at[0, piece(which, i), :], mid, i)

    def mid_mate(i):
        return mate_copy(normed_two.at[0, piece(tp, i), :], normed_two.at[1, piece(tp, i), :], mid, 2 + i)

    def mid_pass(which, i):
        return core_copy(normed_two.at[1, piece(which, i), :], normed_two.at[1, piece(which, i), :], mid, 4 + i)

    for i in range(2):

        @pl.loop(0, strips)
        def _(j, i=i):
            first = i * sub + j * STRIP
            at = pl.ds(pl.multiple_of(first, STRIP), STRIP)
            values = res[at, :]
            factor = lax.rsqrt(jnp.mean(values * values, axis=-1, keepdims=True) + 1e-06)
            normed_two[0, half_rows(tp, first, STRIP), :] = (values * factor * gain_two[...]).astype(jnp.bfloat16)

        mid_mate(i).start()
        mid_core(tp, i).start()
    while todo:
        relay(*todo.pop())
    start_own(DN, 0)
    start_own(DN, 1)


    def feed(seq, at):
        both = mxu(normed_two[seq, at, :], wgu[...])
        gate, up = both[:, :units], both[:, units:]
        hidden[seq, at, :] = (gate / (1.0 + jnp.exp(-gate)) * up).astype(jnp.bfloat16)

    def two_core(index, i):
        return core_copy(
            part_two.at[index, 1, piece(1 - tp, i), :], theirs_two.at[index, 1, halves[i], :], two, index * 5 + i
        )

    def two_mate(index, i):
        return mate_copy(
            outgo_two.at[index, halves[i], :], income_two.at[index, halves[i], :], two, index * 5 + 2 + i
        )

    def two_own(index):
        return core_copy(part_two.at[index, 0, other, :], theirs_two.at[index, 0], two, index * 5 + 4)

    def down(index, i):
        right = wd[index]
        for which in (1 - tp, tp):
            at = piece(which, i)
            part_two[index, 1, at, :] = mxu(hidden[1, at, :], right).astype(jnp.bfloat16)
        two_core(index, i).start()

    def add_cores(index, i):
        two_core(index, i).wait_recv()
        outgo_two[index, halves[i], :] = (
            f32(part_two[index, 1, piece(tp, i), :]) + f32(theirs_two[index, 1, halves[i], :])
        ).astype(jnp.bfloat16)
        two_mate(index, i).start()

    def down_own(index):
        right = wd[index]
        for at in (other, mine):
            part_two[index, 0, at, :] = mxu(hidden[0, at, :], right).astype(jnp.bfloat16)
        two_own(index).start()

    behind = []

    def step(place, i):
        down(order[place], i)
        if behind:
            add_cores(*behind.pop())
        behind.append((order[place], i))

    def flush():
        while behind:
            add_cores(*behind.pop())

    late = sorted((k, rr) for rr in range(2) for k in range(1, n_z))
    late.reverse()

    def relay_down():
        if late:
            k, rr = late.pop()
            relay(DN, rr, k)

    mid_mate(0).wait_recv()
    mid_pass(tp, 0).start()
    x_all(GA)
    x_all(GB)
    relay_down()
    feed(1, piece(tp, 0))
    relay_down()
    mid_pass(1 - tp, 0).wait_recv()
    feed(1, piece(1 - tp, 0))
    local(DN).wait()
    if DN in SHARED:
        x_wait(DN, [(1, 0)])
    step(0, 0)
    step(1, 0)
    flush()
    relay_down()
    mid_mate(1).wait_recv()
    mid_pass(tp, 1).start()
    feed(1, piece(tp, 1))
    mid_pass(1 - tp, 1).wait_recv()
    feed(1, piece(1 - tp, 1))
    step(0, 1)
    step(1, 1)
    flush()
    relay_down()
    for place in (2, 3):
        x_wait(DN, [(place % 2, place // 2)])
        step(place, 0)
        step(place, 1)
    flush()
    feed(0, mine)
    relay_down()
    mid_core(1 - tp, 0).wait_recv()
    mid_core(1 - tp, 1).wait_recv()
    feed(0, other)
    while late:
        relay_down()
    for place in range(4, n_fs):
        x_wait(DN, [(place % 2, place // 2)])
        for i in range(2):
            step(place, i)
        flush()
        down_own(order[place - 4])
    for place in range(n_fs - 4, n_fs):
        down_own(order[place])
    for index in order:
        two_own(index).wait_recv()
        for i in range(2):
            two_mate(index, i).wait_recv()
        cols = pl.ds(pl.multiple_of(index * width, 128), width)
        total = (f32(part_two[index, 0, mine, :]) + f32(theirs_two[index, 0])) + f32(income_two[index])
        final[:, cols] = (res[:, cols] + 0.5 * total).astype(jnp.bfloat16)


    for t in TYPES:
        y_copy(t, fs).wait_send()
        for rr in range(2):
            z_each(t, rr, lambda copy: copy.wait_send())
            for k in range(1, n_z):
                position = kth(k)
                onward = z + jnp.where(position < z, 1, -1)
                x_copy(t, rr, position, rep).wait_send()

                @pl.when(jnp.logical_and(onward >= 0, onward < n_z))
                def _(t=t, rr=rr, position=position, onward=onward):
                    z_fwd(t, rr, position, onward).wait_send()

            if rr == 1 and t in SHARED:
                x_copy(t, 1, z, rep).wait_send()
    sent = [one_core, one_mate, one_pass]
    sent += [make for i in range(2) for make in (mid_core(tp, i), mid_mate(i), mid_pass(tp, i))]
    for index in order:
        sent += [two_own(index), mix_core(index), mix_mate(index), mix_own(index)] + [make(index, i) for i in range(2) for make in (two_core, two_mate)]
    for copy in sent:
        copy.wait_send()


def block(
    n_fs, tokens, mix_gain, w_bgate, w_cgate, w_value, conv_taps, w_mixout, mlp_gain, w_gate, w_up, w_down
):
    rows, dim = tokens.shape
    depth, channels = w_bgate.shape[0], w_bgate.shape[1] // 2
    units = w_gate.shape[1] // 2
    width = w_mixout.shape[1]
    n_z = n_fs // 2
    bf16 = jnp.bfloat16
    hbm = pl.BlockSpec(memory_space=pl.ANY)
    vmem = pl.BlockSpec(memory_space=pltpu.VMEM)
    dma = pltpu.SemaphoreType.DMA
    return pl.pallas_call(
        functools.partial(kernel, n_z),
        out_shape=pltpu.VMEM(tokens.shape, tokens.dtype),
        in_specs=[hbm, vmem, hbm, hbm, hbm, vmem, hbm, vmem, hbm, hbm, hbm],
        out_specs=vmem,
        scratch_shapes=[
            *[pltpu.VMEM((n_fs * depth, channels), bf16)] * 3,
            pltpu.VMEM((n_fs, w_mixout.shape[0] // 2, width), bf16),
            pltpu.VMEM((n_fs * depth, 2 * units), bf16),
            pltpu.VMEM((n_fs, w_down.shape[0] // 2, width), bf16),
            *[pltpu.VMEM((depth, 2 * units), bf16)] * 3,
            pltpu.VMEM((rows, dim), bf16),
            pltpu.VMEM((2, 2 * rows, dim), bf16),
            pltpu.VMEM((2, 2 * rows, channels), jnp.float32),
            pltpu.VMEM((2, 2 * rows, channels), bf16),
            pltpu.VMEM((n_fs, 2, 2 * rows, width), bf16),
            pltpu.VMEM((n_fs, 2, rows, width), bf16),
            pltpu.VMEM((n_fs, rows, width), bf16),
            pltpu.VMEM((n_fs, rows, width), bf16),
            pltpu.VMEM((rows, dim), jnp.float32),
            pltpu.VMEM((2, 2 * rows, dim), bf16),
            pltpu.VMEM((2, 2 * rows, units), bf16),
            pltpu.VMEM((n_fs, 2, 2 * rows, width), bf16),
            pltpu.VMEM((n_fs, 2, rows, width), bf16),
            pltpu.VMEM((n_fs, rows, width), bf16),
            pltpu.VMEM((n_fs, rows, width), bf16),
            pltpu.VMEM((8, channels), jnp.float32),
            dma((8,)),
            *[dma((7,))] * 2,
            dma((7, 2, 2)),
            *[dma((7, 2, n_z))] * 4,
            *[dma((3,))] * 2,
            *[dma((3 * n_fs,))] * 2,
            *[dma((6,))] * 2,
            *[dma((5 * n_fs,))] * 2,
        ],
        compiler_params=pltpu.CompilerParams(
            collective_id=0, has_side_effects=True, vmem_limit_bytes=64_500_000
        ),
    )(
        tokens, mix_gain[None], w_bgate, w_cgate, w_value, conv_taps, w_mixout, mlp_gain[None], w_gate, w_up, w_down
    )


SPECS = (
    P(("rep", "fs", "tp"), None),
    P(),
    P("fs", "tp"),
    P("fs", "tp"),
    P("fs", "tp"),
    P(),
    P("tp", "fs"),
    P(),
    P("fs", "tp"),
    P("fs", "tp"),
    P("tp", "fs"),
)


def permuted(mesh):
    return jax.shard_map(
        build(mesh.shape["fs"]),
        mesh=mesh,
        in_specs=SPECS,
        out_specs=P(("rep", "fs", "tp"), None),
        check_vma=False,
    )


def fused(mesh):
    return jax.shard_map(
        functools.partial(block, mesh.shape["fs"]),
        mesh=mesh,
        in_specs=SPECS,
        out_specs=P(("rep", "fs", "tp"), None),
        check_vma=False,
    )


def solution(mesh):
    n_fs, n_rep, n_tp = (mesh.shape[name] for name in ("fs", "rep", "tp"))

    def step(*operands):
        tokens, w_down = operands[0], operands[-1]
        rows = tokens.shape[0] // (n_rep * n_fs * n_tp)
        width = tokens.shape[1] // n_fs
        units = w_down.shape[0] // n_tp
        aligned = (
            (n_rep, n_tp, n_fs % 2) == (2, 2, 0)
            and (rows % (2 * STRIP), width % LANES, units % (4 * STRIP), units % LANES) == (0, 0, 0, 0)
            and tokens.shape[1] % (4 * LANES) == 0
        )
        return (fused if aligned else permuted)(mesh)(*operands)

    return step
```

time: 198 us -> 177 us (0.89)
  Pallas kernels: 192 us -> 176 us
  local copies, waits for them, and re-layouts: 6.58 us -> 1.06 us
    pallas_call x1, Pallas kernels: 192 us -> 176 us  [block(): pl.pallas_call(functools.partial(kernel, n_z), out_shape=pltpu.VMEM(token...]
    concatenate x1 -> x0, local copies, waits for them, and re-layouts: 2.27 us -> none  [block(): jnp.concatenate([w[:, h * units:(h + 1) * units] for h in range(2) for w...]
where the time goes in v1:
time: 177 us
  Pallas kernels  176 us (99%)
    pallas_call x1, Pallas kernels, block(): pl.pallas_call(functools.partial(kernel, n_z), out_shape=pltpu.VMEM(token...  176 us

profile of v1, /device:TPU:0, one launch (start us, length us, event | category | flops | bytes accessed | tf_op | source)
XLA Modules:
  0.0 176.6 jit_solution(14193399546544904605)
XLA Ops:
  0.0 175.5 %shard_map.109 = bf16[320,2048]{1,0:T(8,128)(2,1)S(1)} custom-call(bf16[320,2048]{1,0:T(8,128)(2,1)} %tok_hbm.1, f32[1,2048]{1,0:T(1,128)} %bitcast.2, bf16[256,1024]{1,0:T(8,128)(2,1)} %wb_hbm.1, bf16[256,1024]{1,0:T(8,128)(2,1)} %wc_hbm.1, bf16[256,1024]{1,0:T(8,128)(2,1)} %wu_hbm.1, f32[3,2048]{1,0:T(4,128)} %taps.1, bf16[1024,256]{1,0:T(8,128)(2,1)} %wo_hbm.1, ...), custom_call_target="tpu_custom_call" | custom-call | tf_op jit(solution)/shard_map/pallas_call | solution.py:674
  175.5 1.1 copy.13

commit v2 on v1

--- a/solution.py
+++ b/solution.py
@@ -154,7 +154,7 @@
 MESH = pl.DeviceIdType.MESH
 STRIP = 16
 LANES = 128
-C, U, B, OUT, GA, GB, DN = TYPES = range(7)
+C, U, B, OUT, *GU, DN = TYPES = range(7)
 SHARED = (DN,)
 
 
@@ -175,7 +175,7 @@
     tok, normed, convolved, gated, part, theirs, outgo, income, res, normed_two, hidden,
     part_two, theirs_two, outgo_two, income_two,
     tail,
-    load_sem, y_send, y_recv, zown_send, zfwd_send, z_recv, x_send, x_recv,
+    load_sem, y_send, y_recv, z_send, z_recv, x_send, x_recv, x_each,
     one_send, one_recv, mix_send, mix_recv, mid_send, mid_recv, two_send, two_recv,
 ):
     rep, fs, tp = (lax.axis_index(name) for name in ("rep", "fs", "tp"))
@@ -208,8 +208,8 @@
         if t in (OUT, DN):
             size = (wo, wd)[t == DN].shape[1] // 2
         else:
-            size = depth // (4 if t in (GA, GB) else 2)
-        first = base + (2 * size if t == GB else 0)
+            size = depth // (2 * len(GU) if t in GU else 2)
+        first = base + (2 * size * GU.index(t) if t in GU else 0)
         if piece is None:
             return pl.ds(pl.multiple_of(first, 16), 2 * size)
         return pl.ds(pl.multiple_of(first + piece * size, 16), size)
@@ -224,7 +224,7 @@
     def slot(t, index, piece=None):
         if t in (OUT, DN):
             return (wo, wd)[t == DN].at[index, rows_of(t, piece, 0), :]
-        return (wc, wu, wb, None, wgu, wgu)[t].at[rows_of(t, piece, index * depth), :]
+        return (wgu if t in GU else (wc, wu, wb)[t]).at[rows_of(t, piece, index * depth), :]
 
     def remote(src, dst, send, recv, device):
         return pltpu.make_async_remote_copy(
@@ -237,23 +237,32 @@
 
     def y_copy(t, index):
         piece = rep if t in SHARED else None
-        src = away.at[rows_of(t, piece, 0), :] if t in (GA, GB) else source(t, 1 - y, piece)
+        src = away.at[rows_of(t, piece, 0), :] if t in GU else source(t, 1 - y, piece)
         return remote(src, slot(t, index, piece), y_send.at[t], y_recv.at[t], mate)
 
     def z_own(t, rr, side):
         index = line(rr, z)
-        src = slot(t, index, rep) if rr == 1 or t in (GA, GB) else source(t, y, rep)
+        src = slot(t, index, rep) if rr == 1 or t in GU else source(t, y, rep)
         return remote(
-            src, slot(t, index, rep), zown_send.at[t, rr, (side + 1) // 2], z_recv.at[t, rr, z], along(z + side)
+            src, slot(t, index, rep), z_send.at[t], z_recv.at[t, rr, z], along(z + side)
         )
 
     def z_fwd(t, rr, position, target):
         place = slot(t, line(rr, position), rep)
-        return remote(place, place, zfwd_send.at[t, rr, position], z_recv.at[t, rr, position], along(target))
-
-    def x_copy(t, rr, position, piece):
+        return remote(place, place, z_send.at[t], z_recv.at[t, rr, position], along(target))
+
+    def x_copy(t, rr, position, piece, own=False):
         place = slot(t, line(rr, position), piece)
-        return remote(place, place, x_send.at[t, rr, position], x_recv.at[t, rr, position], twin)
+        recv = x_each.at[(OUT, DN).index(t), rr, position] if t in (OUT, DN) else x_recv.at[t]
+        return remote(place, place, x_send.at[len(TYPES) if own else t], recv, twin)
+
+    def drain(t, pieces, sem):
+        if t in (OUT, DN):
+            region = (wo, wd)[t == DN].at[pl.ds(0, pieces // 2)]
+        else:
+            size = depth // (2 * len(GU) if t in GU else 2)
+            region = (wgu if t in GU else (wc, wu, wb)[t]).at[pl.ds(0, pieces * size), :]
+        pltpu.make_async_copy(region, region, sem).wait()
 
     def z_each(t, rr, act):
         for side in (-1, 1):
@@ -266,8 +275,11 @@
         if rr == 1:
             y_copy(t, line(1, z)).wait_recv()
             if t in SHARED:
-                x_copy(t, 1, z, rep).start()
+                x_copy(t, 1, z, rep, True).start()
         z_each(t, rr, lambda copy: copy.start())
+
+    inner = jnp.minimum(z, n_z - 1 - z) > 0
+    outer = jnp.logical_not(inner)
 
     def relay(t, rr, k):
         position = kth(k)
@@ -280,22 +292,30 @@
 
         x_copy(t, rr, position, rep).start()
 
+    def relay_if(where, t, rr, ks):
+        @pl.when(where)
+        def _():
+            for k in ks:
+                relay(t, rr, k)
+
+    beyond = range(3, n_z)
+
     def x_wait(t, pairs):
         for rr, k in pairs:
             x_copy(t, rr, kth(k), 1 - rep).wait_recv()
 
     def x_all(t):
-        x_wait(t, [(rr, k) for rr in range(2) for k in range(1, n_z)] + [(1, 0)] * (t in SHARED))
+        drain(t, 2 * (n_z - 1), x_recv.at[t])
 
 
     def half_rows(which, first=0, count=None):
         return pl.ds(pl.multiple_of(which * rows + first, 16), rows if count is None else count)
 
-    def core_copy(src, dst, sems, place):
-        return remote(src, dst, sems[0].at[place], sems[1].at[place], core)
-
-    def mate_copy(src, dst, sems, place):
-        return remote(src, dst, sems[0].at[place], sems[1].at[place], mate)
+    def core_copy(src, dst, sems, place, leave=None):
+        return remote(src, dst, sems[0].at[place if leave is None else leave], sems[1].at[place], core)
+
+    def mate_copy(src, dst, sems, place, leave=None):
+        return remote(src, dst, sems[0].at[place if leave is None else leave], sems[1].at[place], mate)
 
     one, mix, mid, two = (one_send, one_recv), (mix_send, mix_recv), (mid_send, mid_recv), (two_send, two_recv)
     mine, other = half_rows(tp), half_rows(1 - tp)
@@ -315,7 +335,7 @@
 
     raw = [
         pltpu.make_async_copy(src, dst, load_sem.at[place])
-        for src, dst, place in ((tok_hbm, tok, GA), (wg_hbm, raw_gate, GB), (wup_hbm, raw_up, DN + 1))
+        for src, dst, place in ((tok_hbm, tok, GU[0]), (wg_hbm, raw_gate, GU[1]), (wup_hbm, raw_up, len(TYPES)))
     ]
     raw[0].start()
     pl.semaphore_wait(barrier, neighbours)
@@ -372,7 +392,7 @@
             def _(both=both):
                 away[at, :] = both
 
-    for t in (GA, GB, DN):
+    for t in (*GU, DN):
         y_copy(t, fs).start()
 
 
@@ -408,6 +428,8 @@
     start_own(OUT, 1)
     relay(OUT, 0, 1)
     relay(OUT, 1, 1)
+    relay_if(inner, OUT, 0, [2])
+    relay_if(inner, OUT, 1, [2])
     one_mate.wait_recv()
     one_pass.start()
     for t in (C, U):
@@ -415,87 +437,105 @@
         x_all(t)
     core_copy(normed.at[1, other, :], normed.at[1, other, :], one, 2).wait_recv()
 
-    def mix_core(index):
-        return core_copy(part.at[index, 1, other, :], theirs.at[index, 1], mix, index * 3)
-
-    def mix_mate(index):
-        return mate_copy(outgo.at[index], income.at[index], mix, index * 3 + 1)
+    halves = [pl.ds(i * sub, sub) for i in range(2)]
+
+    def piece(which, i):
+        return half_rows(which, i * sub, sub)
+
+    def mix_core(index, i):
+        return core_copy(
+            part.at[index, 1, piece(1 - tp, i), :], theirs.at[index, 1, halves[i], :], mix, index * 4 + i, 0
+        )
+
+    def mix_mate(index, i):
+        return mate_copy(outgo.at[index, halves[i], :], income.at[index, halves[i], :], mix, index * 4 + 2 + i, 1)
 
     def mix_own(index):
-        return core_copy(part.at[index, 0, other, :], theirs.at[index, 0], mix, index * 3 + 2)
-
-    def project_out(index, seq):
+        return core_copy(part.at[index, 0, other, :], theirs.at[index, 0], mix, 4 * n_fs, 2)
+
+    def project_out(index, i):
         right = wo[index]
-        for at in (other, mine):
-            part[index, seq, at, :] = mxu(gated[seq, at, :], right).astype(jnp.bfloat16)
-            if at is other:
-                (mix_own, mix_core)[seq](index).start()
-
-    def send_sum(index):
-        mix_core(index).wait_recv()
-        outgo[index] = (f32(part[index, 1, mine, :]) + f32(theirs[index, 1])).astype(jnp.bfloat16)
-        mix_mate(index).start()
+        for which in (1 - tp, tp):
+            at = piece(which, i)
+            part[index, 1, at, :] = mxu(gated[1, at, :], right).astype(jnp.bfloat16)
+            if which is not tp:
+                mix_core(index, i).start()
+
+    def project_own(index):
+        right = wo[index]
+        part[index, 0, other, :] = mxu(gated[0, other, :], right).astype(jnp.bfloat16)
+        mix_own(index).start()
+        part[index, 0, mine, :] = mxu(gated[0, mine, :], right).astype(jnp.bfloat16)
+
+    def send_sum(index, i):
+        mix_core(index, i).wait_recv()
+        outgo[index, halves[i], :] = (
+            f32(part[index, 1, piece(tp, i), :]) + f32(theirs[index, 1, halves[i], :])
+        ).astype(jnp.bfloat16)
+        mix_mate(index, i).start()
 
     order = [line(rr, kth(k)) for k in range(n_z) for rr in range(2)]
 
+    def mix_out(places, i):
+        places = list(places)
+        for place in places:
+            if i == 0 and place > 1:
+                x_wait(OUT, [(place % 2, place // 2)])
+            project_out(order[place], i)
+            if place > places[0]:
+                send_sum(order[place - 1], i)
+        send_sum(order[places[-1]], i)
+
     convolve(1, 0)
-    relay(OUT, 0, 2)
+    relay_if(outer, OUT, 0, [2])
+    relay_if(inner, OUT, 0, beyond)
     convolve(1, 1)
-    relay(OUT, 1, 2)
+    relay_if(outer, OUT, 1, [2])
+    relay_if(inner, OUT, 1, beyond)
+    for t in GU:
+        start_own(t, 0)
     local(B).wait()
     x_all(B)
     gate_out(1, 0)
     gate_out(1, 1)
     local(OUT).wait()
-    project_out(order[0], 1)
-    project_out(order[1], 1)
-    send_sum(order[0])
-    send_sum(order[1])
-    for k in range(3, n_z):
-        relay(OUT, 0, k)
-        relay(OUT, 1, k)
-    for t in (GA, GB):
-        for rr in range(2):
-            start_own(t, rr)
+    mix_out(range(2), 0)
+    mix_out(range(2, 4), 0)
+    for rr in range(2):
+        relay_if(outer, OUT, rr, beyond)
+    for t in GU:
+        start_own(t, 1)
     core_copy(normed.at[0, other, :], normed.at[0, other, :], one, 0).wait_recv()
-    gu = [(t, rr) for t in (GA, GB) for rr in range(2)]
-    todo = [(*pair, k) for k in range(1, n_z) for pair in gu]
+    todo = [(t, rr, k) for k in range(1, n_z) for rr in range(2) for t in GU]
     todo.reverse()
-    for place in range(2, 2 * n_z):
-        x_wait(OUT, [(place % 2, place // 2)])
-        project_out(order[place], 1)
-        if place > 2:
-            send_sum(order[place - 1])
-        if place % 2 == 1:
+
+    def pump(count):
+        for _ in range(min(count, len(todo))):
             relay(*todo.pop())
-    send_sum(order[-1])
+
+    mix_out(range(4), 1)
+    pump(1)
+    mix_out(range(4, 6), 0)
+    mix_out(range(6, n_fs), 0)
+    pump(1)
+    mix_out(range(4, n_fs), 1)
+    pump(1)
     convolve(0, 0)
-    relay(*todo.pop())
     convolve(0, 1)
+    pump(1)
     gate_out(0, 0)
     gate_out(0, 1)
-    relay(*todo.pop())
     for index in order:
-        project_out(index, 0)
-
-    def add_up(index):
-        mix_own(index).wait_recv()
-        mix_mate(index).wait_recv()
-        cols = pl.ds(pl.multiple_of(index * width, 128), width)
-        res[:, cols] = f32(tok[:, cols]) + (
-            (f32(part[index, 0, mine, :]) + f32(theirs[index, 0])) + f32(income[index])
+        project_own(index)
+
+    def add_up(index, i):
+        mix_mate(index, i).wait_recv()
+        at, cols = halves[i], pl.ds(pl.multiple_of(index * width, 128), width)
+        res[at, cols] = f32(tok[at, cols]) + (
+            (f32(part[index, 0, piece(tp, i), :]) + f32(theirs[index, 0, at, :])) + f32(income[index, at, :])
         )
 
-    relay(*todo.pop())
-    relay(*todo.pop())
-    for index in order:
-        add_up(index)
-
-    halves = [pl.ds(i * sub, sub) for i in range(2)]
     strips = sub // STRIP
-
-    def piece(which, i):
-        return half_rows(which, i * sub, sub)
 
     def mid_core(which, i):
         return core_copy(normed_two.at[0, piece(which, i), :], normed_two.at[0, piece(which, i), :], mid, i)
@@ -506,10 +546,14 @@
     def mid_pass(which, i):
         return core_copy(normed_two.at[1, piece(which, i), :], normed_two.at[1, piece(which, i), :], mid, 4 + i)
 
-    for i in range(2):
+    def norm_two(i):
+        if i == 0:
+            pltpu.make_async_copy(outgo, outgo, mix_recv.at[4 * n_fs]).wait()
+        for index in order:
+            add_up(index, i)
 
         @pl.loop(0, strips)
-        def _(j, i=i):
+        def _(j):
             first = i * sub + j * STRIP
             at = pl.ds(pl.multiple_of(first, STRIP), STRIP)
             values = res[at, :]
@@ -518,8 +562,12 @@
 
         mid_mate(i).start()
         mid_core(tp, i).start()
-    while todo:
-        relay(*todo.pop())
+
+    pump(1)
+    norm_two(0)
+    pump(2)
+    norm_two(1)
+    pump(len(todo))
     start_own(DN, 0)
     start_own(DN, 1)
 
@@ -531,16 +579,16 @@
 
     def two_core(index, i):
         return core_copy(
-            part_two.at[index, 1, piece(1 - tp, i), :], theirs_two.at[index, 1, halves[i], :], two, index * 5 + i
+            part_two.at[index, 1, piece(1 - tp, i), :], theirs_two.at[index, 1, halves[i], :], two, index * 4 + i, 0
         )
 
     def two_mate(index, i):
         return mate_copy(
-            outgo_two.at[index, halves[i], :], income_two.at[index, halves[i], :], two, index * 5 + 2 + i
+            outgo_two.at[index, halves[i], :], income_two.at[index, halves[i], :], two, index * 4 + 2 + i, 1
         )
 
     def two_own(index):
-        return core_copy(part_two.at[index, 0, other, :], theirs_two.at[index, 0], two, index * 5 + 4)
+        return core_copy(part_two.at[index, 0, other, :], theirs_two.at[index, 0], two, 4 * n_fs, 2)
 
     def down(index, i):
         right = wd[index]
@@ -574,21 +622,18 @@
         while behind:
             add_cores(*behind.pop())
 
-    late = sorted((k, rr) for rr in range(2) for k in range(1, n_z))
-    late.reverse()
-
-    def relay_down():
-        if late:
-            k, rr = late.pop()
-            relay(DN, rr, k)
+    def both_down(place):
+        x_wait(DN, [(place % 2, place // 2)])
+        step(place, 0)
+        step(place, 1)
 
     mid_mate(0).wait_recv()
     mid_pass(tp, 0).start()
-    x_all(GA)
-    x_all(GB)
-    relay_down()
+    for t in GU:
+        x_all(t)
+    relay(DN, 0, 1)
     feed(1, piece(tp, 0))
-    relay_down()
+    relay(DN, 1, 1)
     mid_pass(1 - tp, 0).wait_recv()
     feed(1, piece(1 - tp, 0))
     local(DN).wait()
@@ -597,7 +642,7 @@
     step(0, 0)
     step(1, 0)
     flush()
-    relay_down()
+    relay(DN, 0, 2)
     mid_mate(1).wait_recv()
     mid_pass(tp, 1).start()
     feed(1, piece(tp, 1))
@@ -606,29 +651,29 @@
     step(0, 1)
     step(1, 1)
     flush()
-    relay_down()
-    for place in (2, 3):
-        x_wait(DN, [(place % 2, place // 2)])
-        step(place, 0)
-        step(place, 1)
+    relay(DN, 1, 2)
+    both_down(2)
+    both_down(3)
     flush()
+    relay_if(inner, DN, 0, beyond)
     feed(0, mine)
-    relay_down()
+    relay_if(inner, DN, 1, beyond)
+    both_down(4)
+    relay_if(outer, DN, 0, beyond)
+    both_down(5)
+    flush()
     mid_core(1 - tp, 0).wait_recv()
     mid_core(1 - tp, 1).wait_recv()
     feed(0, other)
-    while late:
-        relay_down()
-    for place in range(4, n_fs):
-        x_wait(DN, [(place % 2, place // 2)])
-        for i in range(2):
-            step(place, i)
+    relay_if(outer, DN, 1, beyond)
+    for place in range(6, n_fs):
+        both_down(place)
         flush()
-        down_own(order[place - 4])
-    for place in range(n_fs - 4, n_fs):
+        down_own(order[place - 6])
+    for place in range(n_fs - 6, n_fs):
         down_own(order[place])
+    pltpu.make_async_copy(outgo_two, outgo_two, two_recv.at[4 * n_fs]).wait()
     for index in order:
-        two_own(index).wait_recv()
         for i in range(2):
             two_mate(index, i).wait_recv()
         cols = pl.ds(pl.multiple_of(index * width, 128), width)
@@ -638,23 +683,23 @@
 
     for t in TYPES:
         y_copy(t, fs).wait_send()
-        for rr in range(2):
-            z_each(t, rr, lambda copy: copy.wait_send())
-            for k in range(1, n_z):
-                position = kth(k)
-                onward = z + jnp.where(position < z, 1, -1)
-                x_copy(t, rr, position, rep).wait_send()
-
-                @pl.when(jnp.logical_and(onward >= 0, onward < n_z))
-                def _(t=t, rr=rr, position=position, onward=onward):
-                    z_fwd(t, rr, position, onward).wait_send()
-
-            if rr == 1 and t in SHARED:
-                x_copy(t, 1, z, rep).wait_send()
+        drain(t, 2 * (n_z - 1), x_send.at[t])
+
+        @pl.when(inner)
+        def _(t=t):
+            drain(t, 4 + 2 * (n_z - 1), z_send.at[t])
+
+        @pl.when(outer)
+        def _(t=t):
+            drain(t, 2, z_send.at[t])
+
+        if t in SHARED:
+            x_copy(t, 1, z, rep, True).wait_send()
+    for send, whole in ((mix_send, outgo), (two_send, outgo_two)):
+        for place in range(3):
+            pltpu.make_async_copy(whole, whole, send.at[place]).wait()
     sent = [one_core, one_mate, one_pass]
     sent += [make for i in range(2) for make in (mid_core(tp, i), mid_mate(i), mid_pass(tp, i))]
-    for index in order:
-        sent += [two_own(index), mix_core(index), mix_mate(index), mix_own(index)] + [make(index, i) for i in range(2) for make in (two_core, two_mate)]
     for copy in sent:
         copy.wait_send()
 
@@ -698,14 +743,16 @@
             pltpu.VMEM((n_fs, rows, width), bf16),
             pltpu.VMEM((n_fs, rows, width), bf16),
             pltpu.VMEM((8, channels), jnp.float32),
-            dma((8,)),
-            *[dma((7,))] * 2,
-            dma((7, 2, 2)),
-            *[dma((7, 2, n_z))] * 4,
+            dma((len(TYPES) + 1,)),
+            *[dma((len(TYPES),))] * 3,
+            dma((len(TYPES), 2, n_z)),
+            dma((len(TYPES) + 1,)),
+            dma((len(TYPES),)),
+            dma((2, 2, n_z)),
             *[dma((3,))] * 2,
-            *[dma((3 * n_fs,))] * 2,
+            *[dma((3,)), dma((4 * n_fs + 1,))],
             *[dma((6,))] * 2,
-            *[dma((5 * n_fs,))] * 2,
+            *[dma((3,)), dma((4 * n_fs + 1,))],
         ],
         compiler_params=pltpu.CompilerParams(
             collective_id=0, has_side_effects=True, vmem_limit_bytes=64_500_000

time: 177 us -> 171 us (0.966)
  Pallas kernels: 176 us -> 169 us
    pallas_call x1, Pallas kernels: 176 us -> 169 us  [block(): pl.pallas_call(functools.partial(kernel, n_z), out_shape=pltpu.VMEM(token...]
where the time goes in v2:
time: 171 us
  Pallas kernels  169 us (99%)
    pallas_call x1, Pallas kernels, block(): pl.pallas_call(functools.partial(kernel, n_z), out_shape=pltpu.VMEM(token...  169 us

profile of v2, /device:TPU:0, one launch (start us, length us, event | category | flops | bytes accessed | tf_op | source)
XLA Modules:
  0.0 170.5 jit_solution(15232240680180474261)
XLA Ops:
  0.0 169.5 %shard_map.109 = bf16[320,2048]{1,0:T(8,128)(2,1)S(1)} custom-call(bf16[320,2048]{1,0:T(8,128)(2,1)} %tok_hbm.1, f32[1,2048]{1,0:T(1,128)} %bitcast.2, bf16[256,1024]{1,0:T(8,128)(2,1)} %wb_hbm.1, bf16[256,1024]{1,0:T(8,128)(2,1)} %wc_hbm.1, bf16[256,1024]{1,0:T(8,128)(2,1)} %wu_hbm.1, f32[3,2048]{1,0:T(4,128)} %taps.1, bf16[1024,256]{1,0:T(8,128)(2,1)} %wo_hbm.1, ...), custom_call_target="tpu_custom_call" | custom-call | tf_op jit(solution)/shard_map/pallas_call | solution.py:719
  169.5 1.1 copy.13

commit v3 on v2

--- a/solution.py
+++ b/solution.py
@@ -154,7 +154,7 @@
 MESH = pl.DeviceIdType.MESH
 STRIP = 16
 LANES = 128
-C, U, B, OUT, *GU, DN = TYPES = range(7)
+C, U, B, OUT, *GU, DN = TYPES = range(9)
 SHARED = (DN,)
 
 
@@ -244,12 +244,12 @@
         index = line(rr, z)
         src = slot(t, index, rep) if rr == 1 or t in GU else source(t, y, rep)
         return remote(
-            src, slot(t, index, rep), z_send.at[t], z_recv.at[t, rr, z], along(z + side)
+            src, slot(t, index, rep), z_send.at[t], z_recv.at[t, rr, z - (side < 0)], along(z + side)
         )
 
     def z_fwd(t, rr, position, target):
         place = slot(t, line(rr, position), rep)
-        return remote(place, place, z_send.at[t], z_recv.at[t, rr, position], along(target))
+        return remote(place, place, z_send.at[t], z_recv.at[t, rr, position - (position > target).astype(jnp.int32)], along(target))
 
     def x_copy(t, rr, position, piece, own=False):
         place = slot(t, line(rr, position), piece)
@@ -500,31 +500,39 @@
     gate_out(1, 1)
     local(OUT).wait()
     mix_out(range(2), 0)
+    relay_if(outer, OUT, 0, beyond)
     mix_out(range(2, 4), 0)
-    for rr in range(2):
-        relay_if(outer, OUT, rr, beyond)
+    relay_if(outer, OUT, 1, beyond)
     for t in GU:
         start_own(t, 1)
     core_copy(normed.at[0, other, :], normed.at[0, other, :], one, 0).wait_recv()
     todo = [(t, rr, k) for k in range(1, n_z) for rr in range(2) for t in GU]
-    todo.reverse()
-
-    def pump(count):
-        for _ in range(min(count, len(todo))):
-            relay(*todo.pop())
+    todo = [(inner, todo[::-1]), (outer, todo[::-1])]
+
+    def pump(*counts):
+        for (where, left), count in zip(todo, counts):
+            items = [left.pop() for _ in range(min(count, len(left)))]
+
+            @pl.when(where)
+            def _(items=items):
+                for item in items:
+                    relay(*item)
 
     mix_out(range(4), 1)
-    pump(1)
+    pump(1, 1)
     mix_out(range(4, 6), 0)
+    pump(1, 1)
     mix_out(range(6, n_fs), 0)
-    pump(1)
+    pump(1, 1)
     mix_out(range(4, n_fs), 1)
-    pump(1)
+    pump(2, 2)
     convolve(0, 0)
+    pump(1, 1)
     convolve(0, 1)
-    pump(1)
+    pump(2, 1)
     gate_out(0, 0)
     gate_out(0, 1)
+    pump(3, 1)
     for index in order:
         project_own(index)
 
@@ -546,11 +554,13 @@
     def mid_pass(which, i):
         return core_copy(normed_two.at[1, piece(which, i), :], normed_two.at[1, piece(which, i), :], mid, 4 + i)
 
-    def norm_two(i):
+    def norm_two(i, relays_after):
         if i == 0:
             pltpu.make_async_copy(outgo, outgo, mix_recv.at[4 * n_fs]).wait()
-        for index in order:
+        for place, index in enumerate(order):
             add_up(index, i)
+            if place in relays_after:
+                pump(1, 1)
 
         @pl.loop(0, strips)
         def _(j):
@@ -563,11 +573,12 @@
         mid_mate(i).start()
         mid_core(tp, i).start()
 
-    pump(1)
-    norm_two(0)
-    pump(2)
-    norm_two(1)
-    pump(len(todo))
+    pump(5, 1)
+    norm_two(0, [4])
+    pump(1, 1)
+    norm_two(1, range(n_fs - 1))
+    rest = len(GU) * 2 * (n_z - 1)
+    pump(rest, rest)
     start_own(DN, 0)
     start_own(DN, 1)
 
@@ -745,7 +756,7 @@
             pltpu.VMEM((8, channels), jnp.float32),
             dma((len(TYPES) + 1,)),
             *[dma((len(TYPES),))] * 3,
-            dma((len(TYPES), 2, n_z)),
+            dma((len(TYPES), 2, n_z - 1)),
             dma((len(TYPES) + 1,)),
             dma((len(TYPES),)),
             dma((2, 2, n_z)),

time: 171 us -> 169 us (0.988)
  no operation moved by 1% of the time
where the time goes in v3:
time: 169 us
  Pallas kernels  168 us (99%)
    pallas_call x1, Pallas kernels, block(): pl.pallas_call(functools.partial(kernel, n_z), out_shape=pltpu.VMEM(token...  168 us

profile of v3, /device:TPU:0, one launch (start us, length us, event | category | flops | bytes accessed | tf_op | source)
XLA Modules:
  0.0 169.0 jit_solution(16220074035510003121)
XLA Ops:
  0.0 167.9 %shard_map.109 = bf16[320,2048]{1,0:T(8,128)(2,1)S(1)} custom-call(bf16[320,2048]{1,0:T(8,128)(2,1)} %tok_hbm.1, f32[1,2048]{1,0:T(1,128)} %bitcast.2, bf16[256,1024]{1,0:T(8,128)(2,1)} %wb_hbm.1, bf16[256,1024]{1,0:T(8,128)(2,1)} %wc_hbm.1, bf16[256,1024]{1,0:T(8,128)(2,1)} %wu_hbm.1, f32[3,2048]{1,0:T(4,128)} %taps.1, bf16[1024,256]{1,0:T(8,128)(2,1)} %wo_hbm.1, ...), custom_call_target="tpu_custom_call" | custom-call | tf_op jit(solution)/shard_map/pallas_call | solution.py:730
  167.9 1.1 copy.13

commit v4 on v3

--- a/solution.py
+++ b/solution.py
@@ -574,13 +574,25 @@
         mid_core(tp, i).start()
 
     pump(5, 1)
+
+    def start_down(where):
+        @pl.when(where)
+        def _():
+            for rr in range(2):
+                z_each(DN, rr, lambda copy: copy.start())
+
+    y_copy(DN, line(1, z)).wait_recv()
+    start_down(outer)
     norm_two(0, [4])
     pump(1, 1)
     norm_two(1, range(n_fs - 1))
     rest = len(GU) * 2 * (n_z - 1)
     pump(rest, rest)
-    start_own(DN, 0)
-    start_own(DN, 1)
+    start_down(inner)
+    x_copy(DN, 1, z, rep, True).start()
+    for k in (1, 2):
+        for rr in range(2):
+            relay_if(inner, DN, rr, [k])
 
 
     def feed(seq, at):
@@ -640,11 +652,13 @@
 
     mid_mate(0).wait_recv()
     mid_pass(tp, 0).start()
+    for rr in range(2):
+        relay_if(inner, DN, rr, beyond)
     for t in GU:
         x_all(t)
-    relay(DN, 0, 1)
+    relay_if(outer, DN, 0, [1])
     feed(1, piece(tp, 0))
-    relay(DN, 1, 1)
+    relay_if(outer, DN, 1, [1])
     mid_pass(1 - tp, 0).wait_recv()
     feed(1, piece(1 - tp, 0))
     local(DN).wait()
@@ -653,7 +667,7 @@
     step(0, 0)
     step(1, 0)
     flush()
-    relay(DN, 0, 2)
+    relay_if(outer, DN, 0, [2])
     mid_mate(1).wait_recv()
     mid_pass(tp, 1).start()
     feed(1, piece(tp, 1))
@@ -662,13 +676,11 @@
     step(0, 1)
     step(1, 1)
     flush()
-    relay(DN, 1, 2)
+    relay_if(outer, DN, 1, [2])
     both_down(2)
     both_down(3)
     flush()
-    relay_if(inner, DN, 0, beyond)
     feed(0, mine)
-    relay_if(inner, DN, 1, beyond)
     both_down(4)
     relay_if(outer, DN, 0, beyond)
     both_down(5)

time: 169 us -> 169 us (level)
  no operation moved by 1% of the time
where the time goes in v4:
time: 169 us
  Pallas kernels  168 us (99%)
    pallas_call x1, Pallas kernels, block(): pl.pallas_call(functools.partial(kernel, n_z), out_shape=pltpu.VMEM(token...  168 us

profile of v4, /device:TPU:0, one launch (start us, length us, event | category | flops | bytes accessed | tf_op | source)
XLA Modules:
  0.0 169.0 jit_solution(11135320297022327614)
XLA Ops:
  0.0 167.9 %shard_map.109 = bf16[320,2048]{1,0:T(8,128)(2,1)S(1)} custom-call(bf16[320,2048]{1,0:T(8,128)(2,1)} %tok_hbm.1, f32[1,2048]{1,0:T(1,128)} %bitcast.2, bf16[256,1024]{1,0:T(8,128)(2,1)} %wb_hbm.1, bf16[256,1024]{1,0:T(8,128)(2,1)} %wc_hbm.1, bf16[256,1024]{1,0:T(8,128)(2,1)} %wu_hbm.1, f32[3,2048]{1,0:T(4,128)} %taps.1, bf16[1024,256]{1,0:T(8,128)(2,1)} %wo_hbm.1, ...), custom_call_target="tpu_custom_call" | custom-call | tf_op jit(solution)/shard_map/pallas_call | solution.py:742
  167.9 1.1 copy.13
